TPU v7x, 32 devices: a whole 2x2x4 slice. The times are simulated.
32 devices in a mesh: ep: 8 (over z, core), tp: 4 (over y, x).
Axes of the slice: x: 2, y: 2, z: 4, core: 2. Of those that a mesh axis runs over, the one named last changes fastest.
Arguments:
- tokens: bfloat16 [512, 2048], P('ep', 'tp'), as said below
- mix_gain: float32 [2048], replicated, may hold values from 0.1 to 1.9
- w_in: bfloat16 [2048, 1024], P(None, 'tp'), may hold values from -0.125 to 0.125
- a_real: float32 [64, 64], P('tp'), may hold values from -1 to -0.1
- a_imag: float32 [64, 64], P('tp'), may hold values from -3.140625 to 3.140625
- log_step: float32 [64], P('tp'), may hold values from -3 to 0
- b_coef: float32 [2, 64, 64, 16], P(None, 'tp'), may hold values from -2.5 to 2.5
- output_coefficients: float32 [2, 64, 16, 64], P(None, 'tp'), may hold values from -1.25 to 1.25
- skip: float32 [1024], P('tp'), may hold values from -6 to 6
- w_out: bfloat16 [1024, 2048], P('tp'), may hold values from -0.1875 to 0.1875
- state: float32 [2, 512, 64, 64], P(None, 'ep', 'tp'), may hold values from -6 to 6
- ffn_gain: float32 [2048], replicated, may hold values from 0.1 to 1.9
- w_gate: bfloat16 [16, 2048, 4096], P('ep', None, 'tp'), may hold values from -0.125 to 0.125
- w_up: bfloat16 [16, 2048, 4096], P('ep', None, 'tp'), may hold values from -0.125 to 0.125
- w_down: bfloat16 [16, 4096, 2048], P('ep', 'tp'), may hold values from -0.09375 to 0.09375
- expert_ids: int32 [512, 2], P('ep'), may hold values from 0 to 15, all different within a row; in each aligned block of 64 rows (0 to 63, 64 to 127, ...) at most 16 rows name the same one
- route_weights: float32 [512, 2], P('ep'), may hold values from 0.3 to 1
Outputs:
- out: bfloat16 [512, 2048], P('ep', 'tp')
- new_state: float32 [2, 512, 64, 64], P(None, 'ep', 'tp')
Inputs may be any that keep to these rules, and one draw needn't show every extreme that they name: `expert_ids`: A token's 2 experts differ. Among the 64 rows of one index of ep no expert is named more than 16 times, a bound that some block reaches. `tokens`: feature scales differ along the model width.
All inputs are finite; a program needn't handle non-finite values.
Results may differ from a plain program's by a relative error of at most 0.007.
Values may be sent and summed in bfloat16 or wider, within the bound.
A program may use at most 64 MiB of HBM per device.

v0:
```python
import jax
import jax.numpy as jnp
from jax import lax
from jax.sharding import PartitionSpec as P

epsilon = 1e-06
highest_precision = lax.Precision.HIGHEST


def rms_norm(values, gain):
    scaled = values * lax.rsqrt(jnp.mean(values * values, axis=-1, keepdims=True) + epsilon)
    return scaled * gain


def state_update(drive, a_real, a_imag, log_step, b_coef, output_coefficients, skip, state):
    count = drive.shape[0]
    groups = a_real.shape[0]
    drive_float = drive.astype(jnp.float32)
    grouped = drive_float.reshape(count, groups, -1)
    step_size = jnp.exp(log_step)[:, None]
    magnitude = jnp.exp(step_size * a_real)
    decay_re = magnitude * jnp.cos(step_size * a_imag)
    decay_imaginary = magnitude * jnp.sin(step_size * a_imag)
    denominator = a_real * a_real + a_imag * a_imag
    shifted = decay_re - 1.0
    factor_re = (shifted * a_real + decay_imaginary * a_imag) / denominator
    factor_im = (decay_imaginary * a_real - shifted * a_imag) / denominator
    coef_re = factor_re[..., None] * b_coef[0] - factor_im[..., None] * b_coef[1]
    coefficient_imaginary = factor_re[..., None] * b_coef[1] + factor_im[..., None] * b_coef[0]
    push_re = jnp.einsum("gpc,sgc->sgp", coef_re, grouped, precision=highest_precision)
    push_im = jnp.einsum(
        "gpc,sgc->sgp", coefficient_imaginary, grouped, precision=highest_precision
    )
    state_real = decay_re * state[0] - decay_imaginary * state[1] + push_re
    state_imaginary = decay_re * state[1] + decay_imaginary * state[0] + push_im
    state_readout = jnp.einsum(
        "amz,daz->dam", output_coefficients[0], state_real, precision=highest_precision
    ) - jnp.einsum(
        "amz,daz->dam", output_coefficients[1], state_imaginary, precision=highest_precision
    )
    mixed = state_readout.reshape(count, -1) + skip * drive_float
    return (jax.nn.gelu(mixed).astype(jnp.bfloat16), jnp.stack([state_real, state_imaginary]))


def slot_table(expert_ids, experts, capacity):
    flat_ids = expert_ids.reshape(-1)
    onehot = (flat_ids[:, None] == jnp.arange(experts, dtype=jnp.int32)[None, :]).astype(jnp.int32)
    ranks = jnp.cumsum(onehot, axis=0) - 1
    slot_rank = jnp.sum(onehot * ranks, axis=1)
    slots = flat_ids * capacity + slot_rank
    return (slots[:, None] == jnp.arange(experts * capacity, dtype=jnp.int32)[None, :]).astype(
        jnp.float32
    )


def local(
    tokens,
    mix_gain,
    w_in,
    a_real,
    a_imag,
    log_step,
    b_coef,
    output_coefficients,
    skip,
    w_out,
    state,
    ffn_gain,
    w_gate,
    w_up,
    w_down,
    expert_ids,
    route_weights,
):
    seq_count = tokens.shape[0]
    width = tokens.shape[1]
    top_count = expert_ids.shape[1]
    ep_count = lax.axis_size("ep")
    tp_count = lax.axis_size("tp")
    model_width = width * tp_count
    local_experts = w_gate.shape[0]
    experts = local_experts * ep_count
    capacity = max(2, 2 * seq_count * top_count // experts)
    col_start = lax.axis_index("tp") * width
    whole_rows = lax.all_gather(tokens, "tp", axis=1, tiled=True)
    tok_float = whole_rows.astype(jnp.float32)
    normed = rms_norm(tok_float, mix_gain).astype(jnp.bfloat16)
    drive = jnp.dot(normed, w_in, preferred_element_type=jnp.float32).astype(jnp.bfloat16)
    mixed, new_state = state_update(
        drive, a_real, a_imag, log_step, b_coef, output_coefficients, skip, state
    )
    partial_mix = jnp.dot(mixed, w_out, preferred_element_type=jnp.float32)
    placed = slot_table(expert_ids, experts, capacity)
    per_token = (
        placed.reshape(seq_count, top_count, experts * capacity).sum(axis=1).astype(jnp.bfloat16)
    )
    mix_full = lax.psum(partial_mix, "tp")
    resid_full = (tok_float + mix_full).astype(jnp.bfloat16)
    normed2 = rms_norm(resid_full.astype(jnp.float32), ffn_gain).astype(jnp.bfloat16)
    resid_own = lax.dynamic_slice_in_dim(resid_full, col_start, width, 1)
    send_buffer = jnp.dot(per_token.T, normed2, preferred_element_type=jnp.float32).astype(
        jnp.bfloat16
    )
    send_buffer = send_buffer.reshape(ep_count, local_experts, capacity, model_width)
    slot_rows = lax.all_to_all(send_buffer, "ep", split_axis=0, concat_axis=0, tiled=True)
    gate_vals = jnp.einsum("njcd,jdf->njcf", slot_rows, w_gate, preferred_element_type=jnp.float32)
    up_vals = jnp.einsum("njcd,jdf->njcf", slot_rows, w_up, preferred_element_type=jnp.float32)
    hidden = (jax.nn.silu(gate_vals) * up_vals).astype(jnp.bfloat16)
    partial_out = jnp.einsum("njcf,jfd->njcd", hidden, w_down, preferred_element_type=jnp.float32)
    expert_result = lax.psum_scatter(
        partial_out.astype(jnp.bfloat16), "tp", scatter_dimension=3, tiled=True
    )
    returned_rows = lax.all_to_all(expert_result, "ep", split_axis=0, concat_axis=0, tiled=True)
    returned_rows = returned_rows.reshape(experts * capacity, width).astype(jnp.float32)
    weighted = placed * route_weights.reshape(-1)[:, None]
    combined = jnp.dot(weighted, returned_rows, precision=highest_precision)
    combined = combined.reshape(seq_count, top_count, width).sum(axis=1)
    out = (resid_own.astype(jnp.float32) + combined).astype(jnp.bfloat16)
    return (out, new_state)


def solution(mesh):
    in_specs = (
        P("ep", "tp"),
        P(),
        P(None, "tp"),
        P("tp", None),
        P("tp", None),
        P("tp"),
        P(None, "tp", None, None),
        P(None, "tp", None, None),
        P("tp"),
        P("tp", None),
        P(None, "ep", "tp", None),
        P(),
        P("ep", None, "tp"),
        P("ep", None, "tp"),
        P("ep", "tp", None),
        P("ep", None),
        P("ep", None),
    )
    out_specs = (P("ep", "tp"), P(None, "ep", "tp", None))
    return jax.shard_map(local, mesh=mesh, in_specs=in_specs, out_specs=out_specs, check_vma=False)
```

profile of v0, /device:TPU:0, one launch (start us, length us, event | category | flops | bytes accessed | tf_op | source)
XLA Modules:
  0.0 168.2 jit_solution(7657873128458054456)
XLA Ops:
  7.2 0.0 copy-start
  7.2 0.0 copy-start.1
  7.2 0.0 copy-start.5
  7.2 0.0 copy-start.3
  7.2 0.0 copy-start.2
  7.2 0.0 all-reduce.2.cloned.1.call-start
  7.3 10.9 %all_gather.3 = bf16[64,2048]{1,0:T(8,128)(2,1)S(1)} all-gather(bf16[64,512]{1,0:T(8,128)(2,1)} %param.17), channel_id=1, replica_groups=mesh['ep'=8,'tp'=4] {'tp'}, dimensions={1}, use_global_device_ids=true | all-gather | bytes 327680 | tf_op jit(solution)/shard_map/all_gather | solution.py:85
  18.2 0.2 fusion.31
  18.3 1.6 convolution_convert_fusion.1
  19.9 0.1 copy.68
  20.0 0.7 exp.10
  20.7 1.3 fusion.87
  22.0 0.8 fusion.80
  22.8 1.6 fusion.24
  24.4 1.6 fusion.25
  26.1 1.8 %fusion.43 = f32[16,64,16]{1,2,0:T(8,128)S(1)} fusion(f32[64,16,64]{2,0,1:T(8,128)S(1)} %fusion.25, f32[2,16,16,64]{3,2,1,0:T(8,128)} %param.24), kind=kOutput, calls=%fused_computation.43 | convolution fusion | flops 12582912 | bytes 458752 | tf_op jit(solution)/shard_map/amz,daz->dam/dot_general | solution.py:36
  27.9 0.0 copy-done.1
  27.9 0.9 convolution_subtract_fusion
  28.9 0.1 copy.69
  28.9 0.0 copy-done
  29.0 0.0 copy-done.5
  29.0 1.1 fusion.72
  30.1 0.0 all-reduce.2.cloned.1.call-update
  30.1 0.0 reduce-scatter.2.cloned.1.call-start
  30.1 0.0 copy-done.3
  30.1 0.1 copy.70
  30.2 0.1 eq.49
  30.4 0.1 fusion.67
  30.5 0.2 reduce_window_sum.11
  30.6 0.2 select_reduce_fusion
  30.8 0.1 reduce_sum.49
  31.0 0.1 copy.71
  31.0 0.1 convert_reduce_fusion
  31.2 44.7 %all-reduce.2.cloned.1.call-done = f32[64,2048]{1,0:T(8,128)} async-done(((f32[64,2048]{1,0:T(8,128)}), f32[64,2048]{1,0:T(8,128)}) %all-reduce.2.cloned.1.call-update) | async-done | bytes 524304 | tf_op jit(solution)/shard_map/psum | solution.py:97
  75.9 1.2 fusion.28
  77.1 0.0 copy-done.2
  77.1 0.5 convolution_convert_fusion
  77.6 0.0 slice-start.2
  77.6 31.2 %all_to_all.10 = bf16[8,2,16,2048]{3,2,1,0:T(8,128)(2,1)S(1)} all-to-all(bf16[8,2,16,2048]{3,2,1,0:T(8,128)(2,1)S(1)} %bitcast.107), channel_id=1, replica_groups=mesh['ep'=8,'tp'=4] {'ep'}, dimensions={0} | all-to-all | bytes 2097152 | tf_op jit(solution)/shard_map/all_to_all | solution.py:105
  108.9 0.0 slice-start.3
  108.9 0.0 slice-start
  108.9 4.8 %fusion.12 = f32[8,2,16,1024]{3,2,0,1:T(8,128)S(1)} fusion(bf16[2,2048,1024]{2,1,0:T(8,128)(2,1)} %param.29, bf16[8,2,16,2048]{3,2,1,0:T(8,128)(2,1)S(1)} %all_to_all.10), kind=kOutput, calls=%fused_computation.9 | convolution fusion | flops 1073741824 | bytes 10485760 | tf_op jit(solution)/shard_map/njcd,jdf->njcf/dot_general | solution.py:106
  113.7 0.0 slice-done.2
  113.7 0.0 slice-done.3
  113.7 0.0 slice-start.1
  113.7 1.4 fusion.21
  115.1 0.0 slice-done
  115.1 1.0 slice-done.1
  116.1 0.0 copy-start.4
  116.1 2.2 %fusion.9 = bf16[8,2,16,2048]{3,2,0,1:T(8,128)(2,1)} fusion(bf16[8,2,16,1024]{3,2,0,1:T(8,128)(2,1)S(1)} %fusion.21, bf16[2,1024,2048]{2,1,0:T(8,128)(2,1)S(1)} %bitcast.104), kind=kOutput, calls=%fused_computation.8 | convolution fusion | flops 1074266112 | bytes 9961472 | tf_op jit(solution)/shard_map/njcf,jfd->njcd/dot_general | solution.py:109
  118.4 0.0 reduce-scatter.2.cloned.1.call-update
  118.4 26.0 %reduce-scatter.2.cloned.1.call-done = bf16[8,2,16,512]{3,2,0,1:T(8,128)(2,1)} async-done(((bf16[8,2,16,2048]{3,2,0,1:T(8,128)(2,1)}), bf16[8,2,16,512]{3,2,0,1:T(8,128)(2,1)}) %reduce-scatter.2.cloned.1.call-update) | async-done | bytes 262160 | tf_op jit(solution)/shard_map/reduce_scatter | solution.py:110
  144.4 1.7 copy.74
  146.1 4.6 %all-to-all-start.1 = ((bf16[8,2,16,512]{3,2,1,0:T(8,128)(2,1)}), bf16[8,2,16,512]{3,2,1,0:T(8,128)(2,1)S(1)}, u32[]{:S(2)}, u32[]{:S(2)}) async-start(bf16[8,2,16,512]{3,2,1,0:T(8,128)(2,1)} %copy.74), calls=%async_computation.2 | async-start | bytes 524288 | tf_op jit(solution)/shard_map/all_to_all | solution.py:113
  150.7 0.1 pad_maximum_fusion
  150.8 1.6 copy.75
  152.4 8.0 %all-to-all-done.1 = bf16[8,2,16,512]{3,2,1,0:T(8,128)(2,1)S(1)} async-done(((bf16[8,2,16,512]{3,2,1,0:T(8,128)(2,1)}), bf16[8,2,16,512]{3,2,1,0:T(8,128)(2,1)S(1)}, u32[]{:S(2)}, u32[]{:S(2)}) %all-to-all-start.1) | async-done | bytes 262176 | tf_op jit(solution)/shard_map/all_to_all | solution.py:113
  160.4 0.0 copy-done.4
  160.4 0.3 convolution_reduce_fusion
  160.8 0.7 add_convert_fusion
  (5 shorter events, 0.0 us)
Async XLA Ops:
  7.2 21.8 %copy-start = (bf16[256,2048]{1,0:T(8,128)(2,1)S(1)}, bf16[256,2048]{1,0:T(8,128)(2,1)}, u32[]{:S(2)}) copy-start(bf16[256,2048]{1,0:T(8,128)(2,1)} %param.26) | copy-start | bytes 3145732
  7.2 20.7 %copy-start.1 = (f32[2,16,16,64]{3,2,1,0:T(8,128)S(1)}, f32[2,16,16,64]{3,2,1,0:T(8,128)}, u32[]{:S(2)}) copy-start(f32[2,16,16,64]{3,2,1,0:T(8,128)} %param.24) | copy-start | bytes 393220
  7.2 21.8 %copy-start.5 = (f32[256]{0:T(256)S(1)}, f32[256]{0:T(256)}, u32[]{:S(2)}) copy-start(f32[256]{0:T(256)} %param.25) | copy-start | bytes 3076
  7.2 22.9 %copy-start.3 = (s32[64,2]{0,1:T(2,128)S(1)}, s32[64,2]{0,1:T(2,128)}, u32[]{:S(2)}) copy-start(s32[64,2]{0,1:T(2,128)} %param.32) | copy-start | bytes 1540
  7.2 69.9 %copy-start.2 = (f32[2048]{0:T(1024)S(1)}, f32[2048]{0:T(1024)}, u32[]{:S(2)}) copy-start(f32[2048]{0:T(1024)} %param.28) | copy-start | bytes 24580
  7.2 68.7 %all-reduce.2.cloned.1.call-start = ((), (), s32[]{:S(2)}) async-start(), calls=%async_computation.3 | async-start | bytes 1048576 | tf_op jit(solution)/shard_map/psum | solution.py:97
  30.1 114.4 %reduce-scatter.2.cloned.1.call-start = ((), (), s32[]{:S(2)}) async-start(), calls=%async_computation.4 | async-start | bytes 1310720 | tf_op jit(solution)/shard_map/reduce_scatter | solution.py:110
  77.6 36.0 %slice-start.2 = ((s8[8388608]{0:T(1024)(128)(4,1)}), s8[4194304]{0:T(1024)(128)(4,1)S(1)}, s32[]{:S(2)}) async-start(s8[8388608]{0:T(1024)(128)(4,1)} %bitcast.112), calls=%async_computation.7 | async-start | bytes 8388608
  108.9 4.8 %slice-start.3 = ((s8[8388608]{0:T(1024)(128)(4,1)}), s8[4194304]{0:T(1024)(128)(4,1)S(1)}, s32[]{:S(2)}) async-start(s8[8388608]{0:T(1024)(128)(4,1)} %bitcast.112), calls=%async_computation.8 | async-start | bytes 8388608
  108.9 6.3 %slice-start = ((s8[8388608]{0:T(1024)(128)(4,1)}), s8[4194304]{0:T(1024)(128)(4,1)S(1)}, s32[]{:S(2)}) async-start(s8[8388608]{0:T(1024)(128)(4,1)} %bitcast.103), calls=%async_computation.5 | async-start | bytes 8388608
  113.7 2.5 %slice-start.1 = ((s8[8388608]{0:T(1024)(128)(4,1)}), s8[4194304]{0:T(1024)(128)(4,1)S(1)}, s32[]{:S(2)}) async-start(s8[8388608]{0:T(1024)(128)(4,1)} %bitcast.103), calls=%async_computation.6 | async-start | bytes 8388608
  116.1 44.3 %copy-start.4 = (f32[64,2]{0,1:T(2,128)S(1)}, f32[64,2]{0,1:T(2,128)}, u32[]{:S(2)}) copy-start(f32[64,2]{0,1:T(2,128)} %param.33) | copy-start | bytes 1540
  146.1 14.3 %all-to-all-start.1 = ((bf16[8,2,16,512]{3,2,1,0:T(8,128)(2,1)}), bf16[8,2,16,512]{3,2,1,0:T(8,128)(2,1)S(1)}, u32[]{:S(2)}, u32[]{:S(2)}) async-start(bf16[8,2,16,512]{3,2,1,0:T(8,128)(2,1)} %copy.74), calls=%async_computation.2 | async-start | bytes 524288 | tf_op jit(solution)/shard_map/all_to_all | solution.py:113
Sparse Core Ops, SparseCore 0:
  30.2 45.6 all-reduce.1
  118.5 25.8 reduce-scatter.1
where the time goes:
time: 169 us; the launch traced here: 168 us
  waiting for transfers between devices  78.8 us (47%)
  blocking collectives  42.1 us (25%)
  matrix products  18 us (11%)
  between operations  14.3 us (8%)
  local copies, waits for them, and re-layouts  6.87 us (4%)
  starting transfers between devices  4.69 us (3%)
  other arithmetic  3.53 us (2%)
    psum x1, waiting for transfers between devices, local(): mix_full = lax.psum(partial_mix, 'tp')  44.7 us
    all_to_all x1, blocking collectives, local(): lax.all_to_all(send_buffer, 'ep', split_axis=0, concat_axis=0, tiled=True)  31.2 us
    reduce_scatter x1, waiting for transfers between devices, local(): lax.psum_scatter(partial_out.astype(jnp.bfloat16), 'tp', scatter_dimensio...  26 us
    all_gather x1, blocking collectives, local(): whole_rows = lax.all_gather(tokens, 'tp', axis=1, tiled=True)  10.9 us
    all_to_all x1, waiting for transfers between devices, local(): lax.all_to_all(expert_result, 'ep', split_axis=0, concat_axis=0, tiled=True)  8.01 us
    dot_general x1, matrix products, local(): jnp.einsum('njcd,jdf->njcf', slot_rows, w_gate, preferred_element_type=jn...  4.78 us
    all_to_all x1, starting transfers between devices, local(): lax.all_to_all(expert_result, 'ep', split_axis=0, concat_axis=0, tiled=True)  4.61 us
  transfers between devices with their start and end apart: 3, of which 3 were waited for; matrix products, arithmetic and copies ran while one was open for 2% of the time, Pallas kernels for 0%

commit v1 on v0

--- a/solution.py
+++ b/solution.py
@@ -1,6 +1,10 @@
+import functools
+
 import jax
 import jax.numpy as jnp
 from jax import lax
+from jax.experimental import pallas as pl
+from jax.experimental.pallas import tpu as pltpu
 from jax.sharding import PartitionSpec as P
 
 epsilon = 1e-06
@@ -119,6 +123,426 @@
     return (out, new_state)
 
 
+MESH = pl.DeviceIdType.MESH
+HBM = pltpu.HBM
+
+
+def log2(value):
+    return value.bit_length() - 1
+
+
+def iota(shape, axis):
+    return lax.broadcasted_iota(jnp.int32, shape, axis)
+
+
+def nt_dot(left, right):
+    return lax.dot_general(
+        left, right, (((1,), (1,)), ((), ())), preferred_element_type=jnp.float32
+    )
+
+
+def nn_dot(left, right):
+    return jnp.dot(left, right, preferred_element_type=jnp.float32)
+
+
+def fused_body(
+    sizes,
+    tokens, mix_gain, w_in, a_real, a_imag, log_step, b_coef, out_coef, skip, w_out, state,
+    ffn_gain, w_gate, w_up, w_down, ids, route,
+    out, new_state,
+    tok_v, mg_v, win_v, ar_v, ai_v, ls_v, b_v, oc_v, skip_v, wo_v, st_v, fg_v, wg_v, wu_v, wd_v,
+    ids_v, rw_v,
+    bt_v, ct_v, rows_v, base_v, ns_v, half_v, part_v, part_in, sel_v, pick_v, resid_v, slot_v,
+    x_v, xn_v, hid_v, oo_v, own_v, oo_in, ro_v, ret_v, out_v,
+    load_sem, wload_sem, store_sem,
+    ag_s, ag_r, rs_s, rs_r, dp_s, dp_r, fw_s, fw_r, os_s, os_r, rt_s, rt_r,
+):
+    n_tp, n_ep, seqs, width, groups, states, chans, cap, local_e, hidden = sizes
+    bf16, f32 = jnp.bfloat16, jnp.float32
+    model = width * n_tp
+    lanes = groups * states
+    channels = groups * chans
+    slots = cap * local_e
+    me_t = lax.axis_index("tp")
+    me_e = lax.axis_index("ep")
+
+    def tp_to(d):
+        return lax.rem(me_t + d, n_tp)
+
+    def ep_to(d):
+        return lax.rem(me_e + d, n_ep)
+
+    def ep_from(d):
+        return lax.rem(me_e + n_ep - d, n_ep)
+
+    def remote(src, dst, send, recv, device):
+        return pltpu.make_async_remote_copy(
+            src_ref=src, dst_ref=dst, send_sem=send, recv_sem=recv,
+            device_id=device, device_id_type=MESH,
+        )
+
+    loads = {}
+
+    def load(name, src, dst, sem):
+        copy = pltpu.make_async_copy(src, dst, sem)
+        copy.start()
+        loads[name] = copy
+
+    load("tok", tokens, tok_v.at[me_t], load_sem.at[0])
+    small = (
+        ("ar", a_real, ar_v), ("ai", a_imag, ai_v), ("ls", log_step, ls_v), ("b", b_coef, b_v),
+        ("oc", out_coef, oc_v), ("st", state, st_v), ("mg", mix_gain, mg_v), ("win", w_in, win_v),
+        ("skip", skip, skip_v), ("wo", w_out, wo_v), ("ids", ids, ids_v), ("rw", route, rw_v),
+        ("fg", ffn_gain, fg_v),
+    )
+    for at, (name, src, dst) in enumerate(small):
+        load(name, src, dst, load_sem.at[at + 1])
+
+    barrier = pltpu.get_barrier_semaphore()
+    for d in range(1, n_tp):
+        pl.semaphore_signal(barrier, inc=1, device_id={"tp": tp_to(d)}, device_id_type=MESH)
+    for d in range(1, n_ep):
+        pl.semaphore_signal(barrier, inc=1, device_id={"ep": ep_to(d)}, device_id_type=MESH)
+    loads["tok"].wait()
+    pl.semaphore_wait(barrier, n_tp + n_ep - 2)
+
+    gathers = []
+    for d in range(1, n_tp):
+        copy = remote(
+            tok_v.at[me_t], tok_v.at[me_t], ag_s.at[d - 1], ag_r.at[d - 1], {"tp": tp_to(d)}
+        )
+        copy.start()
+        gathers.append(copy)
+    for j in range(local_e):
+        load(("g", j), w_gate.at[j], wg_v.at[j], wload_sem.at[3 * j])
+        load(("u", j), w_up.at[j], wu_v.at[j], wload_sem.at[3 * j + 1])
+        load(("d", j), w_down.at[j], wd_v.at[j], wload_sem.at[3 * j + 2])
+
+    for name in ("ar", "ai", "ls"):
+        loads[name].wait()
+    log_col = jnp.sum(
+        jnp.where(iota((groups, groups), 0) == iota((groups, groups), 1), ls_v[...], 0.0),
+        axis=1, keepdims=True,
+    )
+    step_size = jnp.exp(log_col)
+    re, im = ar_v[...], ai_v[...]
+    magnitude = jnp.exp(step_size * re)
+    decay_re = magnitude * jnp.cos(step_size * im)
+    decay_im = magnitude * jnp.sin(step_size * im)
+    denominator = re * re + im * im
+    shifted = decay_re - 1.0
+    factor_re = (shifted * re + decay_im * im) / denominator
+    factor_im = (decay_im * re - shifted * im) / denominator
+    spread_state = (
+        jnp.bitwise_and(iota((states, lanes), 1), states - 1) == iota((states, lanes), 0)
+    )
+    own_group = jnp.right_shift(iota((groups, lanes), 1), log2(states)) == iota((groups, lanes), 0)
+    spread_f32 = spread_state.astype(f32)
+    for at, value in enumerate((decay_re, decay_im, factor_re, factor_im)):
+        wide = jnp.dot(
+            value, spread_f32, precision=highest_precision, preferred_element_type=f32
+        )
+        rows_v[pl.ds(at, 1), :] = jnp.sum(jnp.where(own_group, wide, 0.0), axis=0, keepdims=True)
+
+    loads["b"].wait()
+    spread_chan = (
+        jnp.bitwise_and(iota((chans, channels), 1), chans - 1) == iota((chans, channels), 0)
+    ).astype(bf16)
+    b_mask = jnp.right_shift(iota((lanes, channels), 0), log2(states)) == jnp.right_shift(
+        iota((lanes, channels), 1), log2(chans)
+    )
+    for i in range(2):
+        bt_v[i] = jnp.where(b_mask, nn_dot(b_v[i].astype(bf16), spread_chan), 0.0).astype(bf16)
+    loads["oc"].wait()
+    c_mask = jnp.right_shift(iota((channels, lanes), 0), log2(chans)) == jnp.right_shift(
+        iota((channels, lanes), 1), log2(states)
+    )
+    for i in range(2):
+        ct_v[i] = jnp.where(
+            c_mask, nn_dot(oc_v[i].astype(bf16), spread_state.astype(bf16)), 0.0
+        ).astype(bf16)
+
+    loads["st"].wait()
+    pairs = 128 // states
+    for piece in range(groups // pairs):
+        at = pl.ds(piece * 128, 128)
+        old = []
+        for i in range(2):
+            old.append(
+                jnp.concatenate(
+                    [
+                        st_v[i, pl.ds(piece * pairs + k, seqs, stride=groups), :]
+                        for k in range(pairs)
+                    ],
+                    axis=1,
+                )
+            )
+        d_re, d_im = rows_v[pl.ds(0, 1), at], rows_v[pl.ds(1, 1), at]
+        base_v[0, :, at] = d_re * old[0] - d_im * old[1]
+        base_v[1, :, at] = d_re * old[1] + d_im * old[0]
+
+    loads["ids"].wait()
+    experts = n_ep * local_e
+    all_slots = experts * cap
+    chosen = [
+        (ids_v[:, k : k + 1] == iota((seqs, experts), 1)).astype(bf16)
+        for k in range(ids_v.shape[1])
+    ]
+    named = chosen[0]
+    for one in chosen[1:]:
+        named = named + one
+    earlier = (iota((seqs, seqs), 1) < iota((seqs, seqs), 0)).astype(bf16)
+    rank = nn_dot(earlier, named).astype(bf16)
+    tall = (
+        jnp.right_shift(iota((all_slots, experts), 0), log2(cap)) == iota((all_slots, experts), 1)
+    ).astype(bf16)
+    tall_rank = jnp.bitwise_and(iota((all_slots, seqs), 0), cap - 1).astype(f32)
+    hit = (nt_dot(tall, named) > 0.5) & (nt_dot(tall, rank) == tall_rank)
+    sel_v[...] = hit.astype(f32).astype(bf16)
+    wide_rank = jnp.bitwise_and(iota((seqs, all_slots), 1), cap - 1).astype(f32)
+    right_rank = nt_dot(rank, tall) == wide_rank
+    for k, one in enumerate(chosen):
+        pick_v[k] = ((nt_dot(one, tall) > 0.5) & right_rank).astype(f32).astype(bf16)
+
+    loads["mg"].wait()
+    loads["win"].wait()
+    for copy in gathers:
+        copy.wait_recv()
+    square = jnp.zeros((seqs, 1), f32)
+    for t in range(n_tp):
+        value = tok_v[t].astype(f32)
+        square = square + jnp.sum(value * value, axis=1, keepdims=True)
+    scale = lax.rsqrt(square * (1.0 / model) + epsilon)
+    drive = jnp.zeros((seqs, channels), f32)
+    for t in range(n_tp):
+        columns = pl.ds(t * width, width)
+        normed = (tok_v[t].astype(f32) * scale * mg_v[:, columns]).astype(bf16)
+        drive = drive + nn_dot(normed, win_v[columns, :])
+    drive = drive.astype(bf16)
+    push = [nt_dot(drive, bt_v[i]) for i in range(2)]
+    for piece in range(groups // pairs):
+        lo = piece * 128
+        at = pl.ds(lo, 128)
+        f_re, f_im = rows_v[pl.ds(2, 1), at], rows_v[pl.ds(3, 1), at]
+        x_re, x_im = push[0][:, lo : lo + 128], push[1][:, lo : lo + 128]
+        new = (
+            base_v[0, :, at] + (f_re * x_re - f_im * x_im),
+            base_v[1, :, at] + (f_re * x_im + f_im * x_re),
+        )
+        for i in range(2):
+            half_v[i, :, at] = new[i].astype(bf16)
+            base_v[i, :, at] = new[i]
+    readout = nt_dot(half_v[0], ct_v[0]) - nt_dot(half_v[1], ct_v[1])
+    loads["skip"].wait()
+    mixed = jax.nn.gelu(readout + skip_v[...] * drive.astype(f32)).astype(bf16)
+
+    loads["wo"].wait()
+    scatters = []
+    for d in range(1, n_tp):
+        columns = pl.ds(pl.multiple_of(tp_to(d) * width, 128), width)
+        part_v[d - 1] = nn_dot(mixed, wo_v[:, columns]).astype(bf16)
+        copy = remote(
+            part_v.at[d - 1], part_in.at[d - 1], rs_s.at[d - 1], rs_r.at[d - 1], {"tp": tp_to(d)}
+        )
+        copy.start()
+        scatters.append(copy)
+    columns = pl.ds(pl.multiple_of(me_t * width, 128), width)
+    total = nn_dot(mixed, wo_v[:, columns]) + tok_v[me_t].astype(f32)
+    for piece in range(groups // pairs):
+        for i in range(2):
+            for k in range(pairs):
+                ns_v[i, pl.ds(piece * pairs + k, seqs, stride=groups), :] = base_v[
+                    i, :, piece * 128 + k * states : piece * 128 + (k + 1) * states
+                ]
+    keep_state = pltpu.make_async_copy(ns_v, new_state, store_sem.at[0])
+    keep_state.start()
+    for d in range(1, n_tp):
+        scatters[d - 1].wait_recv()
+        total = total + part_in[d - 1].astype(f32)
+    resid = total.astype(bf16)
+    resid_v[...] = resid
+
+    slot_rows = nn_dot(sel_v[...], resid).astype(bf16)
+    slot_v[...] = slot_rows.reshape(n_ep, slots, width)
+    dispatches = {}
+    for d in range(1, n_ep):
+        copy = remote(
+            slot_v.at[ep_to(d)], x_v.at[me_t, me_e], dp_s.at[d - 1], dp_r.at[d - 1],
+            {"ep": ep_to(d)},
+        )
+        copy.start()
+        dispatches[d] = copy
+    x_v[me_t, me_e] = slot_v[me_e]
+    forwards = []
+    for d in range(n_ep):
+        if d:
+            dispatches[d].wait_recv()
+        block = x_v.at[me_t, ep_from(d)]
+        for k in range(1, n_tp):
+            sem = d * (n_tp - 1) + k - 1
+            copy = remote(block, block, fw_s.at[sem], fw_r.at[sem], {"tp": tp_to(k)})
+            copy.start()
+            forwards.append(copy)
+    for copy in forwards:
+        copy.wait_recv()
+
+    loads["fg"].wait()
+    rows = n_ep * cap
+    out_copies = []
+    for j in range(local_e):
+        blocks = [x_v[t, :, pl.ds(j * cap, cap), :].reshape(rows, width) for t in range(n_tp)]
+        square = jnp.zeros((rows, 1), f32)
+        for value in blocks:
+            value = value.astype(f32)
+            square = square + jnp.sum(value * value, axis=1, keepdims=True)
+        scale = lax.rsqrt(square * (1.0 / model) + epsilon)
+        for t in range(n_tp):
+            columns = pl.ds(t * width, width)
+            xn_v[:, columns] = (blocks[t].astype(f32) * scale * fg_v[:, columns]).astype(bf16)
+        loads[("g", j)].wait()
+        loads[("u", j)].wait()
+        tile = 256
+
+        @pl.loop(0, hidden // tile)
+        def _(n, j=j):
+            at = pl.ds(pl.multiple_of(n * tile, tile), tile)
+            gate = nn_dot(xn_v[...], wg_v[j, :, at])
+            up = nn_dot(xn_v[...], wu_v[j, :, at])
+            hid_v[:, at] = (jax.nn.silu(gate) * up).astype(bf16)
+
+        loads[("d", j)].wait()
+        for d in range(1, n_tp):
+            columns = pl.ds(pl.multiple_of(tp_to(d) * width, 128), width)
+            at = j * (n_tp - 1) + d - 1
+            oo_v[at] = nn_dot(hid_v[...], wd_v[j, :, columns]).astype(bf16)
+            copy = remote(oo_v.at[at], oo_in.at[at], os_s.at[at], os_r.at[at], {"tp": tp_to(d)})
+            copy.start()
+            out_copies.append(copy)
+        columns = pl.ds(pl.multiple_of(me_t * width, 128), width)
+        own_v[j] = nn_dot(hid_v[...], wd_v[j, :, columns])
+
+    returns = []
+    for j in range(local_e):
+        total = own_v[j]
+        for d in range(1, n_tp):
+            at = j * (n_tp - 1) + d - 1
+            out_copies[at].wait_recv()
+            total = total + oo_in[at].astype(f32)
+        ro_v[j] = total.astype(bf16).reshape(n_ep, cap, width)
+        for d in range(1, n_ep):
+            at = j * (n_ep - 1) + d - 1
+            copy = remote(
+                ro_v.at[j, ep_to(d)], ret_v.at[me_e, j], rt_s.at[at], rt_r.at[at],
+                {"ep": ep_to(d)},
+            )
+            copy.start()
+            returns.append(copy)
+        ret_v[me_e, j] = ro_v[j, me_e]
+    loads["rw"].wait()
+    for copy in returns:
+        copy.wait_recv()
+    result = resid_v[...].astype(f32)
+    back = ret_v[...].reshape(all_slots, width)
+    for k in range(len(chosen)):
+        result = result + rw_v[:, k : k + 1] * nn_dot(pick_v[k], back)
+    out_v[...] = result.astype(bf16)
+    keep_out = pltpu.make_async_copy(out_v, out, store_sem.at[1])
+    keep_out.start()
+    for copy in gathers + scatters + list(dispatches.values()) + forwards + out_copies + returns:
+        copy.wait_send()
+    keep_state.wait()
+    keep_out.wait()
+
+
+def fused(
+    tokens, mix_gain, w_in, a_real, a_imag, log_step, b_coef, output_coefficients, skip, w_out,
+    state, ffn_gain, w_gate, w_up, w_down, expert_ids, route_weights,
+):
+    bf16, f32 = jnp.bfloat16, jnp.float32
+    n_tp, n_ep = lax.axis_size("tp"), lax.axis_size("ep")
+    seqs, width = tokens.shape
+    groups, states = a_real.shape
+    chans = b_coef.shape[3]
+    local_e, model, hidden = w_gate.shape
+    top = expert_ids.shape[1]
+    experts = local_e * n_ep
+    cap = max(2, 2 * seqs * top // experts)
+    lanes, channels = groups * states, groups * chans
+    slots, rows = cap * local_e, n_ep * cap
+    sizes = (n_tp, n_ep, seqs, width, groups, states, chans, cap, local_e, hidden)
+    args = (
+        tokens, mix_gain[None], w_in, a_real, a_imag, log_step[None],
+        b_coef.reshape(2, lanes, chans), output_coefficients.reshape(2, channels, states),
+        skip[None], w_out, state.reshape(2, seqs * groups, states), ffn_gain[None],
+        w_gate, w_up, w_down, expert_ids, route_weights,
+    )
+    vmem = pltpu.VMEM
+    scratch = [vmem((n_tp, seqs, width), bf16)]
+    scratch += [vmem(a.shape, a.dtype) for a in args[1:]]
+    scratch += [
+        vmem((2, lanes, channels), bf16),
+        vmem((2, channels, lanes), bf16),
+        vmem((8, lanes), f32),
+        vmem((2, seqs, lanes), f32),
+        vmem((2, seqs * groups, states), f32),
+        vmem((2, seqs, lanes), bf16),
+        vmem((n_tp - 1, seqs, width), bf16),
+        vmem((n_tp - 1, seqs, width), bf16),
+        vmem((experts * cap, seqs), bf16),
+        vmem((top, seqs, experts * cap), bf16),
+        vmem((seqs, width), bf16),
+        vmem((n_ep, slots, width), bf16),
+        vmem((n_tp, n_ep, slots, width), bf16),
+        vmem((rows, model), bf16),
+        vmem((rows, hidden), bf16),
+        vmem((local_e * (n_tp - 1), rows, width), bf16),
+        vmem((local_e, rows, width), f32),
+        vmem((local_e * (n_tp - 1), rows, width), bf16),
+        vmem((local_e, n_ep, cap, width), bf16),
+        vmem((n_ep, local_e, cap, width), bf16),
+        vmem((seqs, width), bf16),
+    ]
+    dma = pltpu.SemaphoreType.DMA
+    counts = [14, 3 * local_e, 2]
+    for number in (
+        n_tp - 1, n_tp - 1, n_ep - 1, n_ep * (n_tp - 1), local_e * (n_tp - 1), local_e * (n_ep - 1)
+    ):
+        counts += [number, number]
+    scratch += [dma((number,)) for number in counts]
+    out, new_state = pl.pallas_call(
+        functools.partial(fused_body, sizes),
+        out_shape=(
+            jax.ShapeDtypeStruct((seqs, width), bf16),
+            jax.ShapeDtypeStruct((2, seqs * groups, states), f32),
+        ),
+        in_specs=[pl.BlockSpec(memory_space=HBM)] * len(args),
+        out_specs=(pl.BlockSpec(memory_space=HBM),) * 2,
+        scratch_shapes=scratch,
+        compiler_params=pltpu.CompilerParams(
+            collective_id=0, has_side_effects=True, vmem_limit_bytes=60 * 1024 * 1024
+        ),
+    )(*args)
+    return out, new_state.reshape(state.shape)
+
+
+def fits(mesh_tp, width, groups, states, chans, cap, hidden):
+    powers = all(v & (v - 1) == 0 for v in (states, chans, cap))
+    return (
+        powers and width % 128 == 0 and states <= 128 and groups % max(8, 128 // states) == 0
+        and cap % 16 == 0 and (groups * chans) % 128 == 0 and hidden % 256 == 0
+    )
+
+
+def layer(*args):
+    tokens, a_real, b_coef, w_gate, ids = args[0], args[3], args[6], args[12], args[15]
+    experts = w_gate.shape[0] * lax.axis_size("ep")
+    cap = max(2, 2 * tokens.shape[0] * ids.shape[1] // experts)
+    kernel = fits(
+        lax.axis_size("tp"), tokens.shape[1], *a_real.shape, b_coef.shape[3], cap, w_gate.shape[2]
+    )
+    return fused(*args) if kernel else local(*args)
+
+
 def solution(mesh):
     in_specs = (
         P("ep", "tp"),
@@ -140,4 +564,4 @@
         P("ep", None),
     )
     out_specs = (P("ep", "tp"), P(None, "ep", "tp", None))
-    return jax.shard_map(local, mesh=mesh, in_specs=in_specs, out_specs=out_specs, check_vma=False)
+    return jax.shard_map(layer, mesh=mesh, in_specs=in_specs, out_specs=out_specs, check_vma=False)

time: 169 us -> 61.4 us (0.36)
  waiting for transfers between devices: 78.8 us -> 0 us
  Pallas kernels: 0 us -> 51.7 us
  blocking collectives: 42.1 us -> 0 us
  matrix products: 18 us -> 0 us
  between operations: 14.3 us -> 0.64 us
  starting transfers between devices: 4.69 us -> 0 us
  other arithmetic: 3.53 us -> 0 us
  local copies, waits for them, and re-layouts: 6.87 us -> 8.77 us
    pallas_call x0 -> x1, Pallas kernels: none -> 51.7 us  [fused(): pl.pallas_call(functools.partial(fused_body, sizes), out_shape=(jax.Shape...]
    psum x1 -> x0, waiting for transfers between devices: 44.7 us -> none  [local(): mix_full = lax.psum(partial_mix, 'tp')]
    all_to_all x1 -> x0, blocking collectives: 31.2 us -> none  [local(): lax.all_to_all(send_buffer, 'ep', split_axis=0, concat_axis=0, tiled=True)]
    reduce_scatter x1 -> x0, waiting for transfers between devices: 26 us -> none  [local(): lax.psum_scatter(partial_out.astype(jnp.bfloat16), 'tp', scatter_dimensio...]
    dot_general x11 -> x0, matrix products: 18 us -> none  [the longest x1 4.78 us: local(): jnp.einsum('njcd,jdf->njcf', slot_rows, w_gate, preferred_element_type=jn...]
    all_gather x1 -> x0, blocking collectives: 10.9 us -> none  [local(): whole_rows = lax.all_gather(tokens, 'tp', axis=1, tiled=True)]
    all_to_all x1 -> x0, waiting for transfers between devices: 8.01 us -> none  [local(): lax.all_to_all(expert_result, 'ep', split_axis=0, concat_axis=0, tiled=True)]
    unnamed x22 -> x5, local copies, waits for them, and re-layouts: 2.74 us -> 8.77 us
  transfers between devices with their start and end apart: 3 -> 0, of which waited for: 3 -> 0; matrix products, arithmetic and copies ran while one was open for 2% -> 0% of each run, Pallas kernels for 0% -> 0%
where the time goes in v1:
time: 61.4 us; the launch traced here: 61.1 us
  Pallas kernels  51.7 us (84%)
  local copies, waits for them, and re-layouts  8.77 us (14%)
  between operations  0.64 us (1%)
    pallas_call x1, Pallas kernels, fused(): pl.pallas_call(functools.partial(fused_body, sizes), out_shape=(jax.Shape...  51.7 us
    unnamed x5, local copies, waits for them, and re-layouts  8.77 us

profile of v1, /device:TPU:0, one launch (start us, length us, event | category | flops | bytes accessed | tf_op | source)
XLA Modules:
  0.0 61.1 jit_solution(15967474892560336167)
XLA Ops:
  0.6 1.4 %copy.20.ids = s32[64,2]{1,0:T(8,128)} copy(s32[64,2]{0,1:T(2,128)} %param.32) | data formatting | bytes 1024 | tf_op args[15]
  2.0 1.4 %copy.21.route = f32[64,2]{1,0:T(8,128)} copy(f32[64,2]{0,1:T(2,128)} %param.33) | data formatting | bytes 1024 | tf_op args[16]
  3.4 2.3 %copy.19 = f32[2,16,64,16]{3,2,1,0:T(8,128)} copy(f32[2,16,64,16]{2,3,1,0:T(8,128)} %param.23) | data formatting | bytes 262144 | tf_op args[6]
  5.7 51.7 %shard_map.176 = (bf16[64,512]{1,0:T(8,128)(2,1)}, f32[2,1024,64]{2,1,0:T(8,128)}) custom-call(bf16[64,512]{1,0:T(8,128)(2,1)} %tokens.1, f32[1,2048]{1,0:T(1,128)} %bitcast.12, bf16[2048,256]{1,0:T(8,128)(2,1)} %w_in.1, f32[16,64]{1,0:T(8,128)} %a_real.1, f32[16,64]{1,0:T(8,128)} %a_imag.1, f32[1,16]{1,0:T(1,128)} %bitcast.15, f32[2,1024,16]{2,1,0:T(8,128)} %bitcast.8, ...), custom_call_target="tpu_custom_call" | custom-call | tf_op jit(solution)/shard_map/pallas_call | solution.py:512
  57.4 1.5 %copy.24 = bf16[64,512]{1,0:T(8,128)(2,1)} copy(bf16[64,512]{1,0:T(8,128)(2,1)} %get-tuple-element.8) | data formatting | bytes 131072
  58.8 2.3 %copy.25 = f32[2,64,16,64]{3,2,1,0:T(8,128)} copy(f32[2,64,16,64]{3,2,1,0:T(8,128)} %bitcast.10) | data formatting | bytes 1048576

commit v2 on v1

--- a/solution.py
+++ b/solution.py
@@ -145,6 +145,11 @@
     return jnp.dot(left, right, preferred_element_type=jnp.float32)
 
 
+def to_column(row):
+    shape = (row.shape[1], row.shape[1])
+    return jnp.sum(jnp.where(iota(shape, 0) == iota(shape, 1), row, 0.0), axis=1, keepdims=True)
+
+
 def fused_body(
     sizes,
     tokens, mix_gain, w_in, a_real, a_imag, log_step, b_coef, out_coef, skip, w_out, state,
@@ -162,7 +167,6 @@
     model = width * n_tp
     lanes = groups * states
     channels = groups * chans
-    slots = cap * local_e
     me_t = lax.axis_index("tp")
     me_e = lax.axis_index("ep")
 
@@ -220,11 +224,7 @@
 
     for name in ("ar", "ai", "ls"):
         loads[name].wait()
-    log_col = jnp.sum(
-        jnp.where(iota((groups, groups), 0) == iota((groups, groups), 1), ls_v[...], 0.0),
-        axis=1, keepdims=True,
-    )
-    step_size = jnp.exp(log_col)
+    step_size = jnp.exp(to_column(ls_v[...]))
     re, im = ar_v[...], ai_v[...]
     magnitude = jnp.exp(step_size * re)
     decay_re = magnitude * jnp.cos(step_size * im)
@@ -244,23 +244,14 @@
         )
         rows_v[pl.ds(at, 1), :] = jnp.sum(jnp.where(own_group, wide, 0.0), axis=0, keepdims=True)
 
-    loads["b"].wait()
-    spread_chan = (
-        jnp.bitwise_and(iota((chans, channels), 1), chans - 1) == iota((chans, channels), 0)
-    ).astype(bf16)
-    b_mask = jnp.right_shift(iota((lanes, channels), 0), log2(states)) == jnp.right_shift(
-        iota((lanes, channels), 1), log2(chans)
-    )
-    for i in range(2):
-        bt_v[i] = jnp.where(b_mask, nn_dot(b_v[i].astype(bf16), spread_chan), 0.0).astype(bf16)
-    loads["oc"].wait()
-    c_mask = jnp.right_shift(iota((channels, lanes), 0), log2(chans)) == jnp.right_shift(
+    block = jnp.right_shift(iota((channels, lanes), 0), log2(chans)) == jnp.right_shift(
         iota((channels, lanes), 1), log2(states)
     )
-    for i in range(2):
-        ct_v[i] = jnp.where(
-            c_mask, nn_dot(oc_v[i].astype(bf16), spread_state.astype(bf16)), 0.0
-        ).astype(bf16)
+    spread_bf16 = spread_f32.astype(bf16)
+    for name, src, dst in (("b", b_v, bt_v), ("oc", oc_v, ct_v)):
+        loads[name].wait()
+        for i in range(2):
+            dst[i] = jnp.where(block, nn_dot(src[i].astype(bf16), spread_bf16), 0.0).astype(bf16)
 
     loads["st"].wait()
     pairs = 128 // states
@@ -285,8 +276,10 @@
     experts = n_ep * local_e
     all_slots = experts * cap
     chosen = [
-        (ids_v[:, k : k + 1] == iota((seqs, experts), 1)).astype(bf16)
-        for k in range(ids_v.shape[1])
+        (
+            to_column(ids_v[k : k + 1, :].astype(f32)) == iota((seqs, experts), 1).astype(f32)
+        ).astype(bf16)
+        for k in range(ids_v.shape[0])
     ]
     named = chosen[0]
     for one in chosen[1:]:
@@ -319,7 +312,7 @@
         normed = (tok_v[t].astype(f32) * scale * mg_v[:, columns]).astype(bf16)
         drive = drive + nn_dot(normed, win_v[columns, :])
     drive = drive.astype(bf16)
-    push = [nt_dot(drive, bt_v[i]) for i in range(2)]
+    push = [nn_dot(drive, bt_v[i]) for i in range(2)]
     for piece in range(groups // pairs):
         lo = piece * 128
         at = pl.ds(lo, 128)
@@ -363,34 +356,57 @@
     resid_v[...] = resid
 
     slot_rows = nn_dot(sel_v[...], resid).astype(bf16)
-    slot_v[...] = slot_rows.reshape(n_ep, slots, width)
+    slot_v[...] = slot_rows.reshape(n_ep, local_e, cap, width)
     dispatches = {}
-    for d in range(1, n_ep):
-        copy = remote(
-            slot_v.at[ep_to(d)], x_v.at[me_t, me_e], dp_s.at[d - 1], dp_r.at[d - 1],
-            {"ep": ep_to(d)},
-        )
+    for j in range(local_e):
+        for d in range(1, n_ep):
+            sem = j * (n_ep - 1) + d - 1
+            copy = remote(
+                slot_v.at[ep_to(d), j], x_v.at[j, me_t, me_e], dp_s.at[sem], dp_r.at[sem],
+                {"ep": ep_to(d)},
+            )
+            copy.start()
+            dispatches[j, d] = copy
+    for j in range(local_e):
+        x_v[j, me_t, me_e] = slot_v[me_e, j]
+    beside = (me_t + 1 - 2 * lax.rem(me_t, 2), lax.rem(me_t + 2, n_tp))
+    forwards = {}
+
+    def forward(j, d):
+        if d:
+            dispatches[j, d].wait_recv()
+        block = x_v.at[j, me_t, ep_from(d)]
+        for k in range(2):
+            sem = (j * n_ep + d) * 3 + k
+            copy = remote(block, block, fw_s.at[sem], fw_r.at[sem], {"tp": beside[k]})
+            copy.start()
+            forwards[j, d, k] = copy
+
+    def hand_on(j, d):
+        k = d % 2
+        forwards[j, d, k].wait_recv()
+        block = x_v.at[j, beside[k], ep_from(d)]
+        sem = (j * n_ep + d) * 3 + 2
+        copy = remote(block, block, fw_s.at[sem], fw_r.at[sem], {"tp": beside[1 - k]})
         copy.start()
-        dispatches[d] = copy
-    x_v[me_t, me_e] = slot_v[me_e]
-    forwards = []
+        forwards[j, d, 2] = copy
+
     for d in range(n_ep):
-        if d:
-            dispatches[d].wait_recv()
-        block = x_v.at[me_t, ep_from(d)]
-        for k in range(1, n_tp):
-            sem = d * (n_tp - 1) + k - 1
-            copy = remote(block, block, fw_s.at[sem], fw_r.at[sem], {"tp": tp_to(k)})
-            copy.start()
-            forwards.append(copy)
-    for copy in forwards:
-        copy.wait_recv()
+        forward(0, d)
+    for d in range(n_ep):
+        hand_on(0, d)
+    for j in range(1, local_e):
+        for d in range(n_ep):
+            forward(j, d)
 
     loads["fg"].wait()
     rows = n_ep * cap
     out_copies = []
     for j in range(local_e):
-        blocks = [x_v[t, :, pl.ds(j * cap, cap), :].reshape(rows, width) for t in range(n_tp)]
+        for d in range(n_ep):
+            forwards[j, d, 1 - d % 2].wait_recv()
+            forwards[j, d, 2].wait_recv()
+        blocks = [x_v[j, t].reshape(rows, width) for t in range(n_tp)]
         square = jnp.zeros((rows, 1), f32)
         for value in blocks:
             value = value.astype(f32)
@@ -410,6 +426,9 @@
             up = nn_dot(xn_v[...], wu_v[j, :, at])
             hid_v[:, at] = (jax.nn.silu(gate) * up).astype(bf16)
 
+        if j + 1 < local_e:
+            for d in range(n_ep // 2):
+                hand_on(j + 1, d)
         loads[("d", j)].wait()
         for d in range(1, n_tp):
             columns = pl.ds(pl.multiple_of(tp_to(d) * width, 128), width)
@@ -420,6 +439,9 @@
             out_copies.append(copy)
         columns = pl.ds(pl.multiple_of(me_t * width, 128), width)
         own_v[j] = nn_dot(hid_v[...], wd_v[j, :, columns])
+        if j + 1 < local_e:
+            for d in range(n_ep // 2, n_ep):
+                hand_on(j + 1, d)
 
     returns = []
     for j in range(local_e):
@@ -444,11 +466,13 @@
     result = resid_v[...].astype(f32)
     back = ret_v[...].reshape(all_slots, width)
     for k in range(len(chosen)):
-        result = result + rw_v[:, k : k + 1] * nn_dot(pick_v[k], back)
+        result = result + to_column(rw_v[k : k + 1, :]) * nn_dot(pick_v[k], back)
     out_v[...] = result.astype(bf16)
     keep_out = pltpu.make_async_copy(out_v, out, store_sem.at[1])
     keep_out.start()
-    for copy in gathers + scatters + list(dispatches.values()) + forwards + out_copies + returns:
+    for copy in gathers + scatters + list(dispatches.values()) + list(
+        forwards.values()
+    ) + out_copies + returns:
         copy.wait_send()
     keep_state.wait()
     keep_out.wait()
@@ -468,19 +492,19 @@
     experts = local_e * n_ep
     cap = max(2, 2 * seqs * top // experts)
     lanes, channels = groups * states, groups * chans
-    slots, rows = cap * local_e, n_ep * cap
+    rows = n_ep * cap
     sizes = (n_tp, n_ep, seqs, width, groups, states, chans, cap, local_e, hidden)
     args = (
         tokens, mix_gain[None], w_in, a_real, a_imag, log_step[None],
-        b_coef.reshape(2, lanes, chans), output_coefficients.reshape(2, channels, states),
+        b_coef.transpose(0, 1, 3, 2).reshape(2, channels, states), output_coefficients.reshape(2, channels, states),
         skip[None], w_out, state.reshape(2, seqs * groups, states), ffn_gain[None],
-        w_gate, w_up, w_down, expert_ids, route_weights,
+        w_gate, w_up, w_down, expert_ids.T, route_weights.T,
     )
     vmem = pltpu.VMEM
     scratch = [vmem((n_tp, seqs, width), bf16)]
     scratch += [vmem(a.shape, a.dtype) for a in args[1:]]
     scratch += [
-        vmem((2, lanes, channels), bf16),
+        vmem((2, channels, lanes), bf16),
         vmem((2, channels, lanes), bf16),
         vmem((8, lanes), f32),
         vmem((2, seqs, lanes), f32),
@@ -491,8 +515,8 @@
         vmem((experts * cap, seqs), bf16),
         vmem((top, seqs, experts * cap), bf16),
         vmem((seqs, width), bf16),
-        vmem((n_ep, slots, width), bf16),
-        vmem((n_tp, n_ep, slots, width), bf16),
+        vmem((n_ep, local_e, cap, width), bf16),
+        vmem((local_e, n_tp, n_ep, cap, width), bf16),
         vmem((rows, model), bf16),
         vmem((rows, hidden), bf16),
         vmem((local_e * (n_tp - 1), rows, width), bf16),
@@ -505,7 +529,8 @@
     dma = pltpu.SemaphoreType.DMA
     counts = [14, 3 * local_e, 2]
     for number in (
-        n_tp - 1, n_tp - 1, n_ep - 1, n_ep * (n_tp - 1), local_e * (n_tp - 1), local_e * (n_ep - 1)
+        n_tp - 1, n_tp - 1, local_e * (n_ep - 1), local_e * n_ep * 3, local_e * (n_tp - 1),
+        local_e * (n_ep - 1),
     ):
         counts += [number, number]
     scratch += [dma((number,)) for number in counts]
@@ -522,13 +547,50 @@
             collective_id=0, has_side_effects=True, vmem_limit_bytes=60 * 1024 * 1024
         ),
     )(*args)
+    out, new_state = hand_over(out, new_state)
     return out, new_state.reshape(state.shape)
+
+
+def hand_over_body(out, new_state, out_to, state_to, out_v, state_v, sems):
+    pieces = [(out, out_v, out_to)]
+    part = new_state.shape[1] // 2
+    for i in range(2):
+        for k in range(2):
+            at = (i, pl.ds(k * part, part))
+            pieces.append((new_state.at[at], state_v.at[at], state_to.at[at]))
+    reads = [
+        pltpu.make_async_copy(src, mid, sems.at[0, n]) for n, (src, mid, _) in enumerate(pieces)
+    ]
+    writes = [
+        pltpu.make_async_copy(mid, dst, sems.at[1, n]) for n, (_, mid, dst) in enumerate(pieces)
+    ]
+    for copy in reads:
+        copy.start()
+    for read, write in zip(reads, writes):
+        read.wait()
+        write.start()
+    for copy in writes:
+        copy.wait()
+
+
+def hand_over(out, new_state):
+    return pl.pallas_call(
+        hand_over_body,
+        out_shape=tuple(jax.ShapeDtypeStruct(a.shape, a.dtype) for a in (out, new_state)),
+        in_specs=[pl.BlockSpec(memory_space=HBM)] * 2,
+        out_specs=(pl.BlockSpec(memory_space=HBM),) * 2,
+        scratch_shapes=[
+            pltpu.VMEM(out.shape, out.dtype),
+            pltpu.VMEM(new_state.shape, new_state.dtype),
+            pltpu.SemaphoreType.DMA((2, 5)),
+        ],
+    )(out, new_state)
 
 
 def fits(mesh_tp, width, groups, states, chans, cap, hidden):
     powers = all(v & (v - 1) == 0 for v in (states, chans, cap))
     return (
-        powers and width % 128 == 0 and states <= 128 and groups % max(8, 128 // states) == 0
+        powers and mesh_tp == 4 and width % 128 == 0 and states <= 128 and groups % max(8, 128 // states) == 0
         and cap % 16 == 0 and (groups * chans) % 128 == 0 and hidden % 256 == 0
     )
 

time: 61.4 us -> 56.4 us (0.919)
  local copies, waits for them, and re-layouts: 8.77 us -> 0 us
  Pallas kernels: 51.7 us -> 55.6 us
    unnamed x5 -> x0, local copies, waits for them, and re-layouts: 8.77 us -> none
    pallas_call x0 -> x1, Pallas kernels: none -> 2.04 us  [hand_over(): pl.pallas_call(hand_over_body, out_shape=tuple((jax.ShapeDtypeStruct(a.sh...]
    pallas_call x1, Pallas kernels: 51.7 us -> 53.5 us  [fused(): pl.pallas_call(functools.partial(fused_body, sizes), out_shape=(jax.Shape...]
where the time goes in v2:
time: 56.4 us; the launch traced here: 56.2 us
  Pallas kernels  55.6 us (99%)
  between operations  0.65 us (1%)
    pallas_call x1, Pallas kernels, fused(): pl.pallas_call(functools.partial(fused_body, sizes), out_shape=(jax.Shape...  53.5 us
    pallas_call x1, Pallas kernels, hand_over(): pl.pallas_call(hand_over_body, out_shape=tuple((jax.ShapeDtypeStruct(a.sh...  2.04 us

profile of v2, /device:TPU:0, one launch (start us, length us, event | category | flops | bytes accessed | tf_op | source)
XLA Modules:
  0.0 56.2 jit_solution(11167392927015373044)
XLA Ops:
  0.6 53.5 %shard_map.176 = (bf16[64,512]{1,0:T(8,128)(2,1)}, f32[2,1024,64]{2,1,0:T(8,128)}) custom-call(bf16[64,512]{1,0:T(8,128)(2,1)} %tokens.1, f32[1,2048]{1,0:T(1,128)} %bitcast.15, bf16[2048,256]{1,0:T(8,128)(2,1)} %w_in.1, f32[16,64]{1,0:T(8,128)} %a_real.1, f32[16,64]{1,0:T(8,128)} %a_imag.1, f32[1,16]{1,0:T(1,128)} %bitcast.20, f32[2,256,64]{2,1,0:T(8,128)} %bitcast.13, ...), custom_call_target="tpu_custom_call" | custom-call | tf_op jit(solution)/shard_map/pallas_call | solution.py:537
  54.2 2.0 %shard_map.177 = (bf16[64,512]{1,0:T(8,128)(2,1)}, f32[2,1024,64]{2,1,0:T(8,128)}) custom-call(bf16[64,512]{1,0:T(8,128)(2,1)} %get-tuple-element.6.out, f32[2,1024,64]{2,1,0:T(8,128)} %get-tuple-element.7.new_state), custom_call_target="tpu_custom_call" | custom-call | tf_op jit(solution)/shard_map/pallas_call | solution.py:577
